TPU v7x, 32 devices: a whole 2x2x4 slice. The times are simulated.
32 devices in a mesh: sp: 8 (over z, x), tp: 4 (over y, core).
Axes of the slice: x: 2, y: 2, z: 4, core: 2. Of those that a mesh axis runs over, the one named last changes fastest.
Arguments:
- inputs: bfloat16 [4096, 2048], P('sp', 'tp'), may hold values from -45 to 45
- norm_gain: float32 [3, 2048], replicated, may hold values from 0.1 to 1.9
- w_value: bfloat16 [3, 2048, 1024], P(None, 'sp', 'tp'), may hold values from -0.125 to 0.125
- w_gate: bfloat16 [3, 2048, 1024], P(None, 'sp', 'tp'), may hold values from -0.125 to 0.125
- conv_taps: float32 [3, 31, 1024], P(None, None, 'tp'), may hold values from -5 to 5
- ln_gain: float32 [3, 1024], P(None, 'tp'), may hold values from 0.1 to 1.9
- ln_bias: float32 [3, 1024], P(None, 'tp'), may hold values from -3 to 3
- w_out: bfloat16 [3, 1024, 2048], P(None, 'tp', 'sp'), may hold values from -0.1875 to 0.1875
Outputs:
- stream: bfloat16 [4096, 2048], P('sp', 'tp')
All inputs are finite; a program needn't handle non-finite values.
Results may differ from a plain program's by a relative error of at most 0.01.
Values may be sent and summed in bfloat16 or wider, within the bound.
A program may use at most 64 MiB of HBM per device.

v0:
```python
import jax
import jax.numpy as jnp
from jax import lax
from jax.sharding import PartitionSpec as P


def from_behind(block, axis, distance):
    devices = range(lax.axis_size(axis))
    route = [(i - distance, i) for i in devices if i - distance in devices]
    return lax.ppermute(block, axis, route)


def shards(inputs, norm_gain, w_value, w_gate, conv_taps, ln_gain, ln_bias, w_out):
    rows = inputs.shape[0]
    reach = conv_taps.shape[1] - 1
    layers = conv_taps.shape[0]
    channels = conv_taps.shape[2] * lax.axis_size("tp")
    whole_value, whole_gate, whole_out = (
        lax.all_gather(w_value, "sp", axis=1, tiled=True),
        lax.all_gather(w_gate, "sp", axis=1, tiled=True),
        lax.all_gather(w_out, "sp", axis=2, tiled=True),
    )
    stream = inputs
    for layer in range(layers):
        full_rows = lax.all_gather(stream, "tp", axis=1, tiled=True)
        xf = full_rows.astype(jnp.float32)
        meansq = jnp.mean(xf * xf, axis=1, keepdims=True)
        hidden = (xf * lax.rsqrt(meansq + 1e-06) * norm_gain[layer][None, :]).astype(jnp.bfloat16)
        value = jnp.dot(hidden, whole_value[layer], preferred_element_type=jnp.float32)
        gate = jnp.dot(hidden, whole_gate[layer], preferred_element_type=jnp.float32)
        glu = (value * jax.nn.sigmoid(gate)).astype(jnp.bfloat16)
        rim = from_behind(glu[rows - reach :], "sp", 1)
        padded = jnp.concatenate([rim, glu], axis=0)
        count = padded.shape[0] - reach
        filtered = jnp.zeros((count, glu.shape[1]), jnp.float32)
        for tap in range(reach + 1):
            filtered = filtered + conv_taps[layer, tap][None, :] * padded[tap : tap + count].astype(
                jnp.float32
            )
        total_sum, total_sq = lax.psum(
            (jnp.sum(filtered, axis=1), jnp.sum(filtered * filtered, axis=1)), "tp"
        )
        mean_val = (total_sum / channels)[:, None]
        var_val = (total_sq / channels)[:, None] - mean_val * mean_val
        normed = jax.nn.silu(
            (filtered - mean_val) * lax.rsqrt(var_val + 1e-06) * ln_gain[layer][None, :]
            + ln_bias[layer][None, :]
        ).astype(jnp.bfloat16)
        partial_out = jnp.dot(normed, whole_out[layer], preferred_element_type=jnp.float32)
        summed = lax.psum_scatter(
            partial_out.astype(jnp.bfloat16), "tp", scatter_dimension=1, tiled=True
        ).astype(jnp.float32)
        kept = stream.astype(jnp.float32)
        stream = (kept + summed).astype(jnp.bfloat16)
    return stream


def solution(mesh):
    in_specs = (
        P("sp", "tp"),
        P(),
        P(None, "sp", "tp"),
        P(None, "sp", "tp"),
        P(None, None, "tp"),
        P(None, "tp"),
        P(None, "tp"),
        P(None, "tp", "sp"),
    )
    out_specs = P("sp", "tp")
    return jax.shard_map(shards, mesh=mesh, in_specs=in_specs, out_specs=out_specs, check_vma=False)
```

profile of v0, /device:TPU:0, one launch (start us, length us, event | category | flops | bytes accessed | tf_op | source)
XLA Modules:
  0.0 422.9 jit_solution(3484355526385756584)
XLA Ops:
  13.1 21.1 %all-gather.7.cloned.1.call-done = bf16[512,2048]{1,0:T(8,128)(2,1)} async-done(((bf16[512,512]{1,0:T(8,128)(2,1)}), bf16[512,2048]{1,0:T(8,128)(2,1)}) %all-gather.7.cloned.1.call-update) | async-done | bytes 2097168 | tf_op jit(solution)/shard_map/all_gather | solution.py:25
  34.2 2.1 fusion
  36.3 60.1 %all-gather.11.cloned.1.call-done = bf16[3,2048,256]{2,1,0:T(8,128)(2,1)} async-done(((bf16[3,256,256]{2,1,0:T(8,128)(2,1)}), bf16[3,2048,256]{2,1,0:T(8,128)(2,1)}) %all-gather.11.cloned.1.call-update) | async-done | bytes 3145744 | tf_op jit(solution)/shard_map/all_gather | solution.py:20
  96.4 2.8 fusion.17
  99.2 58.1 %all-gather.9.cloned.1.call-done = bf16[3,2048,256]{2,1,0:T(8,128)(2,1)} async-done(((bf16[3,256,256]{2,1,0:T(8,128)(2,1)}), bf16[3,2048,256]{2,1,0:T(8,128)(2,1)}) %all-gather.9.cloned.1.call-update) | async-done | bytes 3145744 | tf_op jit(solution)/shard_map/all_gather | solution.py:19
  157.4 2.0 fusion.18
  159.4 2.5 collective-permute-start
  163.3 2.4 fusion.134
  165.7 5.7 %all-reduce.2 = (f32[512]{0:T(512)S(1)}, f32[512]{0:T(512)S(1)}) all-reduce(f32[512]{0:T(512)S(1)} %get-tuple-element.10, f32[512]{0:T(512)S(1)} %get-tuple-element.9), channel_id=1, replica_groups=mesh['sp'=8,'tp'=4] {'tp'}, use_global_device_ids=true, to_apply=%region_4.0 | all-reduce | flops 1024 | bytes 8192 | tf_op jit(solution)/shard_map/psum | solution.py:40
  171.4 49.2 %all-gather.13.cloned.1.call-done = bf16[3,256,2048]{2,1,0:T(8,128)(2,1)} async-done(((bf16[3,256,256]{2,1,0:T(8,128)(2,1)}), bf16[3,256,2048]{2,1,0:T(8,128)(2,1)}) %all-gather.13.cloned.1.call-update) | async-done | bytes 3145744 | tf_op jit(solution)/shard_map/all_gather | solution.py:21
  220.6 3.4 convolution_convert_fusion.2
  224.1 29.5 %reduce-scatter.4.cloned.1.call-done = bf16[512,512]{1,0:T(8,128)(2,1)} async-done(((bf16[512,2048]{1,0:T(8,128)(2,1)}), bf16[512,512]{1,0:T(8,128)(2,1)}) %reduce-scatter.4.cloned.1.call-update) | async-done | bytes 524304 | tf_op jit(solution)/shard_map/reduce_scatter | solution.py:50
  253.6 2.0 add_convert_fusion.2
  255.6 22.6 %all-gather.15.cloned.1.call-done = bf16[512,2048]{1,0:T(8,128)(2,1)} async-done(((bf16[512,512]{1,0:T(8,128)(2,1)}), bf16[512,2048]{1,0:T(8,128)(2,1)}) %all-gather.15.cloned.1.call-update) | async-done | bytes 2097168 | tf_op jit(solution)/shard_map/all_gather | solution.py:25
  278.3 2.1 fusion.3
  280.4 2.8 fusion.14
  283.2 2.0 fusion.19
  285.2 3.4 collective-permute-start.1
  290.0 2.4 fusion.133
  292.4 6.0 %all-reduce.1 = (f32[512]{0:T(512)S(1)}, f32[512]{0:T(512)S(1)}) all-reduce(f32[512]{0:T(512)S(1)} %get-tuple-element.8, f32[512]{0:T(512)S(1)} %get-tuple-element.7), channel_id=1, replica_groups=mesh['sp'=8,'tp'=4] {'tp'}, use_global_device_ids=true, to_apply=%region_10.11 | all-reduce | flops 1024 | bytes 8192 | tf_op jit(solution)/shard_map/psum | solution.py:40
  298.4 3.4 convolution_convert_fusion.1
  301.9 32.1 %reduce-scatter.6.cloned.1.call-done = bf16[512,512]{1,0:T(8,128)(2,1)} async-done(((bf16[512,2048]{1,0:T(8,128)(2,1)}), bf16[512,512]{1,0:T(8,128)(2,1)}) %reduce-scatter.6.cloned.1.call-update) | async-done | bytes 524304 | tf_op jit(solution)/shard_map/reduce_scatter | solution.py:50
  334.0 2.0 add_convert_fusion.1
  336.0 22.7 %all-gather.17.cloned.1.call-done = bf16[512,2048]{1,0:T(8,128)(2,1)} async-done(((bf16[512,512]{1,0:T(8,128)(2,1)}), bf16[512,2048]{1,0:T(8,128)(2,1)}) %all-gather.17.cloned.1.call-update) | async-done | bytes 2097168 | tf_op jit(solution)/shard_map/all_gather | solution.py:25
  358.7 2.1 fusion.6
  360.8 2.8 fusion.11
  363.6 2.0 fusion.20
  365.6 3.6 collective-permute-start.2
  370.4 2.4 fusion.132
  372.8 5.9 %all-reduce = (f32[512]{0:T(512)S(1)}, f32[512]{0:T(512)S(1)}) all-reduce(f32[512]{0:T(512)S(1)} %get-tuple-element.6, f32[512]{0:T(512)S(1)} %get-tuple-element.5), channel_id=1, replica_groups=mesh['sp'=8,'tp'=4] {'tp'}, use_global_device_ids=true, to_apply=%region_16.17 | all-reduce | flops 1024 | bytes 8192 | tf_op jit(solution)/shard_map/psum | solution.py:40
  378.8 3.4 convolution_convert_fusion
  382.2 32.1 %reduce-scatter.8.cloned.1.call-done = bf16[512,512]{1,0:T(8,128)(2,1)} async-done(((bf16[512,2048]{1,0:T(8,128)(2,1)}), bf16[512,512]{1,0:T(8,128)(2,1)}) %reduce-scatter.8.cloned.1.call-update) | async-done | bytes 524304 | tf_op jit(solution)/shard_map/reduce_scatter | solution.py:50
  (55 shorter events, 12.9 us)
Async XLA Ops:
  6.5 27.7 %all-gather.7.cloned.1.call-start = ((), (), s32[]{:S(2)}) async-start(), calls=%async_computation.3 | async-start | bytes 2621440 | tf_op jit(solution)/shard_map/all_gather | solution.py:25
  7.3 89.2 %all-gather.11.cloned.1.call-start = ((), (), s32[]{:S(2)}) async-start(), calls=%async_computation.5 | async-start | bytes 3538944 | tf_op jit(solution)/shard_map/all_gather | solution.py:20
  8.0 149.3 %all-gather.9.cloned.1.call-start = ((), (), s32[]{:S(2)}) async-start(), calls=%async_computation.4 | async-start | bytes 3538944 | tf_op jit(solution)/shard_map/all_gather | solution.py:19
  8.7 211.9 %all-gather.13.cloned.1.call-start = ((), (), s32[]{:S(2)}) async-start(), calls=%async_computation.6 | async-start | bytes 3538944 | tf_op jit(solution)/shard_map/all_gather | solution.py:21
  9.3 244.2 %reduce-scatter.4.cloned.1.call-start = ((), (), s32[]{:S(2)}) async-start(), calls=%async_computation.7 | async-start | bytes 2621440 | tf_op jit(solution)/shard_map/reduce_scatter | solution.py:50
  96.4 60.9 %copy-start.3 = (bf16[512,2048]{1,0:T(8,128)(2,1)S(1)}, bf16[512,2048]{1,0:T(8,128)(2,1)}, u32[]{:S(2)}) copy-start(bf16[512,2048]{1,0:T(8,128)(2,1)} %all-gather.7.cloned.1.call-done) | copy-start | bytes 6291460
  99.2 62.6 %copy-start.7 = (f32[3,256]{1,0:T(4,128)S(1)}, f32[3,256]{1,0:T(4,128)}, u32[]{:S(2)}) copy-start(f32[3,256]{1,0:T(4,128)} %param.14) | copy-start | bytes 9220
  159.4 3.9 collective-permute-start
  220.6 33.0 %copy-start.2 = (bf16[512,512]{1,0:T(8,128)(2,1)S(1)}, bf16[512,512]{1,0:T(8,128)(2,1)}, u32[]{:S(2)}) copy-start(bf16[512,512]{1,0:T(8,128)(2,1)} %param.8) | copy-start | bytes 1572868
  224.0 31.6 %copy-start.6 = (f32[3,31,256]{2,1,0:T(8,128)S(1)}, f32[3,31,256]{2,1,0:T(8,128)}, u32[]{:S(2)}) copy-start(f32[3,31,256]{2,1,0:T(8,128)} %param.12) | copy-start | bytes 285700
  224.0 54.3 %all-gather.15.cloned.1.call-start = ((), (), s32[]{:S(2)}) async-start(), calls=%async_computation.8 | async-start | bytes 2621440 | tf_op jit(solution)/shard_map/all_gather | solution.py:25
  255.6 78.4 %reduce-scatter.6.cloned.1.call-start = ((), (), s32[]{:S(2)}) async-start(), calls=%async_computation.9 | async-start | bytes 2621440 | tf_op jit(solution)/shard_map/reduce_scatter | solution.py:50
  280.4 2.8 copy-start.4
  285.2 4.8 %collective-permute-start.1 = (bf16[30,256]{1,0:T(8,128)(2,1)S(1)}, bf16[30,256]{1,0:T(8,128)(2,1)S(1)}, u32[]{:S(2)}, u32[]{:S(2)}) collective-permute-start(bf16[30,256]{1,0:T(8,128)(2,1)S(1)} %slice.880), channel_id=1, source_target_pairs={{0,4},{4,8},{8,12},{12,16},{16,20},{20,24},{24,28},{1,5},{5,9},{9,... | collective-permute-start | bytes 46088 | tf_op jit(solution)/shard_map/ppermute | solution.py:10
  298.4 35.5 %copy-start = (bf16[512,512]{1,0:T(8,128)(2,1)S(1)}, bf16[512,512]{1,0:T(8,128)(2,1)}, u32[]{:S(2)}) copy-start(bf16[512,512]{1,0:T(8,128)(2,1)} %add_convert_fusion.2) | copy-start | bytes 1572868
  301.8 56.8 %all-gather.17.cloned.1.call-start = ((), (), s32[]{:S(2)}) async-start(), calls=%async_computation.10 | async-start | bytes 2621440 | tf_op jit(solution)/shard_map/all_gather | solution.py:25
  336.0 78.4 %reduce-scatter.8.cloned.1.call-start = ((), (), s32[]{:S(2)}) async-start(), calls=%async_computation.11 | async-start | bytes 2621440 | tf_op jit(solution)/shard_map/reduce_scatter | solution.py:50
  360.8 2.8 copy-start.5
  365.6 4.8 %collective-permute-start.2 = (bf16[30,256]{1,0:T(8,128)(2,1)S(1)}, bf16[30,256]{1,0:T(8,128)(2,1)S(1)}, u32[]{:S(2)}, u32[]{:S(2)}) collective-permute-start(bf16[30,256]{1,0:T(8,128)(2,1)S(1)} %slice.942), channel_id=1, source_target_pairs={{0,4},{4,8},{8,12},{12,16},{16,20},{20,24},{24,28},{1,5},{5,9},{9,... | collective-permute-start | bytes 46088 | tf_op jit(solution)/shard_map/ppermute | solution.py:10
  378.8 35.6 %copy-start.1 = (bf16[512,512]{1,0:T(8,128)(2,1)S(1)}, bf16[512,512]{1,0:T(8,128)(2,1)}, u32[]{:S(2)}) copy-start(bf16[512,512]{1,0:T(8,128)(2,1)} %add_convert_fusion.1) | copy-start | bytes 1572868
Sparse Core Ops, SparseCore 0:
  8.9 25.2 all-gather.6
  36.4 60.0 all-gather.10
  98.6 58.6 all-gather.8
  159.2 61.3 all-gather.12
  224.1 29.3 reduce-scatter.3
  255.7 22.5 all-gather.14
  302.0 31.9 reduce-scatter.5
  336.1 22.5 all-gather.16
  382.4 31.9 reduce-scatter.7
where the time goes:
time: 424 us; the launch traced here: 423 us
  waiting for transfers between devices  334 us (79%)
  matrix products  24.6 us (6%)
  other arithmetic  19.5 us (5%)
  blocking collectives  17.6 us (4%)
  between operations  13.4 us (3%)
  starting transfers between devices  9.7 us (2%)
    reduce_scatter x3, waiting for transfers between devices, shards(): lax.psum_scatter(partial_out.astype(jnp.bfloat16), 'tp', scatter_dimensio...  93.7 us
    all_gather x3, waiting for transfers between devices, shards(): full_rows = lax.all_gather(stream, 'tp', axis=1, tiled=True)  66.4 us
    all_gather x1, waiting for transfers between devices, shards(): lax.all_gather(w_gate, 'sp', axis=1, tiled=True)  60.1 us
    all_gather x1, waiting for transfers between devices, shards(): lax.all_gather(w_value, 'sp', axis=1, tiled=True)  58.1 us
    all_gather x1, waiting for transfers between devices, shards(): lax.all_gather(w_out, 'sp', axis=2, tiled=True)  49.2 us
    psum x3, blocking collectives, shards(): lax.psum((jnp.sum(filtered, axis=1), jnp.sum(filtered * filtered, axis=1)...  17.6 us
    dot_general x3, matrix products, shards(): jnp.dot(normed, whole_out[layer], preferred_element_type=jnp.float32)  10.2 us
    ppermute x3, starting transfers between devices, from_behind(): return lax.ppermute(block, axis, route)  9.38 us
  transfers between devices with their start and end apart: 12, of which 12 were waited for; matrix products, arithmetic and copies ran while one was open for 3% of the time, Pallas kernels for 0%

commit v1 on v0

--- a/solution.py
+++ b/solution.py
@@ -22,7 +22,14 @@
     )
     stream = inputs
     for layer in range(layers):
-        full_rows = lax.all_gather(stream, "tp", axis=1, tiled=True)
+        ring = [stream]
+        for hop in range(3):
+            ring.append(lax.ppermute(ring[-1], "tp", [(dev, (dev + 1) % 4) for dev in range(4)]))
+        full_rows = jnp.roll(
+            jnp.concatenate(ring[::-1], axis=1),
+            (lax.axis_index("tp") + 1) * ring[0].shape[1],
+            axis=1,
+        )
         xf = full_rows.astype(jnp.float32)
         meansq = jnp.mean(xf * xf, axis=1, keepdims=True)
         hidden = (xf * lax.rsqrt(meansq + 1e-06) * norm_gain[layer][None, :]).astype(jnp.bfloat16)

time: 424 us -> 410 us (0.967)
  waiting for transfers between devices: 334 us -> 313 us
  other arithmetic: 19.5 us -> 28.8 us
    ppermute x0 -> x9, waiting for transfers between devices: none -> 74.1 us  [shards(): lax.ppermute(ring[-1], 'tp', [(dev, (dev + 1) % 4) for dev in range(4)])]
    all_gather x3 -> x0, waiting for transfers between devices: 66.4 us -> none  [shards(): full_rows = lax.all_gather(stream, 'tp', axis=1, tiled=True)]
    all_gather x1, waiting for transfers between devices: 60.1 us -> 30.8 us  [shards(): lax.all_gather(w_gate, 'sp', axis=1, tiled=True)]
    reduce_sum x3, other arithmetic: 6.22 us -> 17.2 us  [shards(): meansq = jnp.mean(xf * xf, axis=1, keepdims=True)]
  transfers between devices with their start and end apart: 12 -> 18, of which waited for: 12 -> 18; matrix products, arithmetic and copies ran while one was open for 3% -> 4% of each run, Pallas kernels for 0% -> 0%
where the time goes in v1:
time: 410 us; the launch traced here: 409 us
  waiting for transfers between devices  313 us (76%)
  other arithmetic  28.8 us (7%)
  matrix products  22.2 us (5%)
  blocking collectives  17.6 us (4%)
  between operations  13.7 us (3%)
  starting transfers between devices  10.3 us (3%)
    reduce_scatter x3, waiting for transfers between devices, shards(): lax.psum_scatter(partial_out.astype(jnp.bfloat16), 'tp', scatter_dimensio...  93.7 us
    ppermute x9, waiting for transfers between devices, shards(): lax.ppermute(ring[-1], 'tp', [(dev, (dev + 1) % 4) for dev in range(4)])  74.1 us
    all_gather x1, waiting for transfers between devices, shards(): lax.all_gather(w_value, 'sp', axis=1, tiled=True)  58.9 us
    all_gather x1, waiting for transfers between devices, shards(): lax.all_gather(w_out, 'sp', axis=2, tiled=True)  49.4 us
    all_gather x1, waiting for transfers between devices, shards(): lax.all_gather(w_gate, 'sp', axis=1, tiled=True)  30.8 us
    psum x3, blocking collectives, shards(): lax.psum((jnp.sum(filtered, axis=1), jnp.sum(filtered * filtered, axis=1)...  17.6 us
    reduce_sum x3, other arithmetic, shards(): meansq = jnp.mean(xf * xf, axis=1, keepdims=True)  17.2 us
    dot_general x3, matrix products, shards(): jnp.dot(normed, whole_out[layer], preferred_element_type=jnp.float32)  10.1 us
  transfers between devices with their start and end apart: 18, of which 18 were waited for; matrix products, arithmetic and copies ran while one was open for 4% of the time, Pallas kernels for 0%

profile of v1, /device:TPU:0, one launch (start us, length us, event | category | flops | bytes accessed | tf_op | source)
XLA Modules:
  0.0 409.4 jit_solution(12010405297522412371)
XLA Ops:
  9.3 9.0 %collective-permute-done = bf16[512,512]{1,0:T(8,128)(2,1)S(1)} collective-permute-done((bf16[512,512]{1,0:T(8,128)(2,1)}, bf16[512,512]{1,0:T(8,128)(2,1)S(1)}, u32[]{:S(2)}, u32[]{:S(2)}) %collective-permute-start) | collective-permute-done | bytes 524320 | tf_op jit(solution)/shard_map/ppermute | solution.py:27
  20.5 6.5 %collective-permute-done.1 = bf16[512,512]{1,0:T(8,128)(2,1)S(1)} collective-permute-done((bf16[512,512]{1,0:T(8,128)(2,1)S(1)}, bf16[512,512]{1,0:T(8,128)(2,1)S(1)}, u32[]{:S(2)}, u32[]{:S(2)}) %collective-permute-start.1) | collective-permute-done | bytes 524320 | tf_op jit(solution)/shard_map/ppermute | solution.py:27
  28.7 7.0 %collective-permute-done.2 = bf16[512,512]{1,0:T(8,128)(2,1)} collective-permute-done((bf16[512,512]{1,0:T(8,128)(2,1)S(1)}, bf16[512,512]{1,0:T(8,128)(2,1)}, u32[]{:S(2)}, u32[]{:S(2)}) %collective-permute-start.2) | collective-permute-done | bytes 524320 | tf_op jit(solution)/shard_map/ppermute | solution.py:27
  35.7 5.8 %fusion = (f32[512]{0:T(512)S(1)}, bf16[512,2048]{1,0:T(8,128)(2,1)S(1)}) fusion(s32[]{:T(128)S(6)} %select_n.15, bf16[512,512]{1,0:T(8,128)(2,1)} %param.10, bf16[512,512]{1,0:T(8,128)(2,1)S(1)} %collective-permute-done, bf16[512,512]{1,0:T(8,128)(2,1)S(1)} %collective-permute-done.1, bf16[512,512]{1,0:T(8,128)(2,1)} %collective-permute-done.2), kind=kLoop, calls=%fused_computation.6 | loop fusion | flops 19922432 | bytes 4196356 | tf_op jit(solution)/shard_map/reduce_sum | solution.py:34
  41.5 30.8 %all-gather.6.cloned.1.call-done = bf16[3,2048,256]{2,1,0:T(8,128)(2,1)} async-done(((bf16[3,256,256]{2,1,0:T(8,128)(2,1)}), bf16[3,2048,256]{2,1,0:T(8,128)(2,1)}) %all-gather.6.cloned.1.call-update) | async-done | bytes 3145744 | tf_op jit(solution)/shard_map/all_gather | solution.py:20
  72.3 2.0 fusion.38
  74.3 58.9 %all-gather.4.cloned.1.call-done = bf16[3,2048,256]{2,1,0:T(8,128)(2,1)} async-done(((bf16[3,256,256]{2,1,0:T(8,128)(2,1)}), bf16[3,2048,256]{2,1,0:T(8,128)(2,1)}) %all-gather.4.cloned.1.call-update) | async-done | bytes 3145744 | tf_op jit(solution)/shard_map/all_gather | solution.py:19
  135.2 2.5 collective-permute-start.3
  139.1 2.4 fusion.155
  141.5 5.7 %all-reduce.2 = (f32[512]{0:T(512)S(1)}, f32[512]{0:T(512)S(1)}) all-reduce(f32[512]{0:T(512)S(1)} %get-tuple-element.11, f32[512]{0:T(512)S(1)} %get-tuple-element.10), channel_id=1, replica_groups=mesh['sp'=8,'tp'=4] {'tp'}, use_global_device_ids=true, to_apply=%region_4.6 | all-reduce | flops 1024 | bytes 8192 | tf_op jit(solution)/shard_map/psum | solution.py:47
  147.2 49.4 %all-gather.8.cloned.1.call-done = bf16[3,256,2048]{2,1,0:T(8,128)(2,1)} async-done(((bf16[3,256,256]{2,1,0:T(8,128)(2,1)}), bf16[3,256,2048]{2,1,0:T(8,128)(2,1)}) %all-gather.8.cloned.1.call-update) | async-done | bytes 3145744 | tf_op jit(solution)/shard_map/all_gather | solution.py:21
  196.6 3.4 convolution_convert_fusion.2
  200.1 29.5 %reduce-scatter.4.cloned.1.call-done = bf16[512,512]{1,0:T(8,128)(2,1)} async-done(((bf16[512,2048]{1,0:T(8,128)(2,1)}), bf16[512,512]{1,0:T(8,128)(2,1)}) %reduce-scatter.4.cloned.1.call-update) | async-done | bytes 524304 | tf_op jit(solution)/shard_map/reduce_scatter | solution.py:57
  230.8 8.6 %collective-permute-done.4 = bf16[512,512]{1,0:T(8,128)(2,1)S(1)} collective-permute-done((bf16[512,512]{1,0:T(8,128)(2,1)S(1)}, bf16[512,512]{1,0:T(8,128)(2,1)S(1)}, u32[]{:S(2)}, u32[]{:S(2)}) %collective-permute-start.4) | collective-permute-done | bytes 524320 | tf_op jit(solution)/shard_map/ppermute | solution.py:27
  239.4 8.6 %collective-permute-done.5 = bf16[512,512]{1,0:T(8,128)(2,1)S(1)} collective-permute-done((bf16[512,512]{1,0:T(8,128)(2,1)S(1)}, bf16[512,512]{1,0:T(8,128)(2,1)S(1)}, u32[]{:S(2)}, u32[]{:S(2)}) %collective-permute-start.5) | collective-permute-done | bytes 524320 | tf_op jit(solution)/shard_map/ppermute | solution.py:27
  248.0 8.6 %collective-permute-done.6 = bf16[512,512]{1,0:T(8,128)(2,1)S(1)} collective-permute-done((bf16[512,512]{1,0:T(8,128)(2,1)S(1)}, bf16[512,512]{1,0:T(8,128)(2,1)S(1)}, u32[]{:S(2)}, u32[]{:S(2)}) %collective-permute-start.6) | collective-permute-done | bytes 524320 | tf_op jit(solution)/shard_map/ppermute | solution.py:27
  256.6 5.7 %fusion.3 = (f32[512]{0:T(512)S(1)}, bf16[512,2048]{1,0:T(8,128)(2,1)S(1)}) fusion(s32[]{:T(128)S(6)} %select_n.15, bf16[512,512]{1,0:T(8,128)(2,1)S(1)} %add_convert_fusion.2, bf16[512,512]{1,0:T(8,128)(2,1)S(1)} %collective-permute-done.4, bf16[512,512]{1,0:T(8,128)(2,1)S(1)} %collective-permute-done.5, bf16[512,512]{1,0:T(8,128)(2,1)S(1)} %collective-permute-done.6), kind=kLoop, calls=%fused_computation.9 | loop fusion | flops 19922432 | bytes 4196356 | tf_op jit(solution)/shard_map/reduce_sum | solution.py:34
  266.4 3.4 collective-permute-start.7
  271.1 2.4 fusion.154
  273.6 6.0 %all-reduce.1 = (f32[512]{0:T(512)S(1)}, f32[512]{0:T(512)S(1)}) all-reduce(f32[512]{0:T(512)S(1)} %get-tuple-element.9, f32[512]{0:T(512)S(1)} %get-tuple-element.8), channel_id=1, replica_groups=mesh['sp'=8,'tp'=4] {'tp'}, use_global_device_ids=true, to_apply=%region_10.12 | all-reduce | flops 1024 | bytes 8192 | tf_op jit(solution)/shard_map/psum | solution.py:47
  279.6 3.4 convolution_convert_fusion.1
  283.0 32.1 %reduce-scatter.6.cloned.1.call-done = bf16[512,512]{1,0:T(8,128)(2,1)} async-done(((bf16[512,2048]{1,0:T(8,128)(2,1)}), bf16[512,512]{1,0:T(8,128)(2,1)}) %reduce-scatter.6.cloned.1.call-update) | async-done | bytes 524304 | tf_op jit(solution)/shard_map/reduce_scatter | solution.py:57
  316.3 8.6 %collective-permute-done.8 = bf16[512,512]{1,0:T(8,128)(2,1)S(1)} collective-permute-done((bf16[512,512]{1,0:T(8,128)(2,1)S(1)}, bf16[512,512]{1,0:T(8,128)(2,1)S(1)}, u32[]{:S(2)}, u32[]{:S(2)}) %collective-permute-start.8) | collective-permute-done | bytes 524320 | tf_op jit(solution)/shard_map/ppermute | solution.py:27
  324.9 8.6 %collective-permute-done.9 = bf16[512,512]{1,0:T(8,128)(2,1)S(1)} collective-permute-done((bf16[512,512]{1,0:T(8,128)(2,1)S(1)}, bf16[512,512]{1,0:T(8,128)(2,1)S(1)}, u32[]{:S(2)}, u32[]{:S(2)}) %collective-permute-start.9) | collective-permute-done | bytes 524320 | tf_op jit(solution)/shard_map/ppermute | solution.py:27
  333.5 8.6 %collective-permute-done.10 = bf16[512,512]{1,0:T(8,128)(2,1)S(1)} collective-permute-done((bf16[512,512]{1,0:T(8,128)(2,1)S(1)}, bf16[512,512]{1,0:T(8,128)(2,1)S(1)}, u32[]{:S(2)}, u32[]{:S(2)}) %collective-permute-start.10) | collective-permute-done | bytes 524320 | tf_op jit(solution)/shard_map/ppermute | solution.py:27
  342.1 5.7 %fusion.6 = (f32[512]{0:T(512)S(1)}, bf16[512,2048]{1,0:T(8,128)(2,1)S(1)}) fusion(s32[]{:T(128)S(6)} %select_n.15, bf16[512,512]{1,0:T(8,128)(2,1)S(1)} %add_convert_fusion.1, bf16[512,512]{1,0:T(8,128)(2,1)S(1)} %collective-permute-done.8, bf16[512,512]{1,0:T(8,128)(2,1)S(1)} %collective-permute-done.9, bf16[512,512]{1,0:T(8,128)(2,1)S(1)} %collective-permute-done.10), kind=kLoop, calls=%fused_computation.12 | loop fusion | flops 19922432 | bytes 4196356 | tf_op jit(solution)/shard_map/reduce_sum | solution.py:34
  347.8 2.0 fusion.32
  351.9 3.6 collective-permute-start.11
  356.7 2.4 fusion.153
  359.1 5.9 %all-reduce = (f32[512]{0:T(512)S(1)}, f32[512]{0:T(512)S(1)}) all-reduce(f32[512]{0:T(512)S(1)} %get-tuple-element.7, f32[512]{0:T(512)S(1)} %get-tuple-element.6), channel_id=1, replica_groups=mesh['sp'=8,'tp'=4] {'tp'}, use_global_device_ids=true, to_apply=%region_16.18 | all-reduce | flops 1024 | bytes 8192 | tf_op jit(solution)/shard_map/psum | solution.py:47
  365.1 3.4 convolution_convert_fusion
  368.5 32.1 %reduce-scatter.8.cloned.1.call-done = bf16[512,512]{1,0:T(8,128)(2,1)} async-done(((bf16[512,2048]{1,0:T(8,128)(2,1)}), bf16[512,512]{1,0:T(8,128)(2,1)}) %reduce-scatter.8.cloned.1.call-update) | async-done | bytes 524304 | tf_op jit(solution)/shard_map/reduce_scatter | solution.py:57
  (54 shorter events, 23.2 us)
Async XLA Ops:
  6.5 65.8 %all-gather.6.cloned.1.call-start = ((), (), s32[]{:S(2)}) async-start(), calls=%async_computation.4 | async-start | bytes 3538944 | tf_op jit(solution)/shard_map/all_gather | solution.py:20
  7.3 125.9 %all-gather.4.cloned.1.call-start = ((), (), s32[]{:S(2)}) async-start(), calls=%async_computation.3 | async-start | bytes 3538944 | tf_op jit(solution)/shard_map/all_gather | solution.py:19
  8.0 188.6 %all-gather.8.cloned.1.call-start = ((), (), s32[]{:S(2)}) async-start(), calls=%async_computation.5 | async-start | bytes 3538944 | tf_op jit(solution)/shard_map/all_gather | solution.py:21
  8.7 220.8 %reduce-scatter.4.cloned.1.call-start = ((), (), s32[]{:S(2)}) async-start(), calls=%async_computation.6 | async-start | bytes 2621440 | tf_op jit(solution)/shard_map/reduce_scatter | solution.py:57
  8.8 9.6 %collective-permute-start = (bf16[512,512]{1,0:T(8,128)(2,1)}, bf16[512,512]{1,0:T(8,128)(2,1)S(1)}, u32[]{:S(2)}, u32[]{:S(2)}) collective-permute-start(bf16[512,512]{1,0:T(8,128)(2,1)} %param.10), channel_id=1, source_target_pairs={{0,1},{1,2},{2,3},{3,0},{4,5},{5,6},{6,7},{7,4},{8,9},{9,10},{10,1... | collective-permute-start | bytes 1572872 | tf_op jit(solution)/shard_map/ppermute | solution.py:27
  18.4 8.6 %collective-permute-start.1 = (bf16[512,512]{1,0:T(8,128)(2,1)S(1)}, bf16[512,512]{1,0:T(8,128)(2,1)S(1)}, u32[]{:S(2)}, u32[]{:S(2)}) collective-permute-start(bf16[512,512]{1,0:T(8,128)(2,1)S(1)} %collective-permute-done), channel_id=1, source_target_pairs={{0,1},{1,2},{2,3},{3,0},{4,5},{5,6},{6,7},{7,4},{8,9},{9,10},{10,1... | collective-permute-start | bytes 1572872 | tf_op jit(solution)/shard_map/ppermute | solution.py:27
  27.0 8.7 %collective-permute-start.2 = (bf16[512,512]{1,0:T(8,128)(2,1)S(1)}, bf16[512,512]{1,0:T(8,128)(2,1)}, u32[]{:S(2)}, u32[]{:S(2)}) collective-permute-start(bf16[512,512]{1,0:T(8,128)(2,1)S(1)} %collective-permute-done.1), channel_id=1, source_target_pairs={{0,1},{1,2},{2,3},{3,0},{4,5},{5,6},{6,7},{7,4},{8,9},{9,10},{10,1... | collective-permute-start | bytes 1572872 | tf_op jit(solution)/shard_map/ppermute | solution.py:27
  74.3 63.4 %copy-start.2 = (f32[3,256]{1,0:T(4,128)S(1)}, f32[3,256]{1,0:T(4,128)}, u32[]{:S(2)}) copy-start(f32[3,256]{1,0:T(4,128)} %param.16) | copy-start | bytes 9220
  135.2 3.9 collective-permute-start.3
  196.6 33.0 %copy-start = (bf16[512,512]{1,0:T(8,128)(2,1)S(1)}, bf16[512,512]{1,0:T(8,128)(2,1)}, u32[]{:S(2)}) copy-start(bf16[512,512]{1,0:T(8,128)(2,1)} %param.10) | copy-start | bytes 1572868
  200.0 48.0 %copy-start.1 = (f32[3,31,256]{2,1,0:T(8,128)S(1)}, f32[3,31,256]{2,1,0:T(8,128)}, u32[]{:S(2)}) copy-start(f32[3,31,256]{2,1,0:T(8,128)} %param.14) | copy-start | bytes 285700
  200.0 115.0 %reduce-scatter.6.cloned.1.call-start = ((), (), s32[]{:S(2)}) async-start(), calls=%async_computation.7 | async-start | bytes 2621440 | tf_op jit(solution)/shard_map/reduce_scatter | solution.py:57
  230.7 8.7 %collective-permute-start.4 = (bf16[512,512]{1,0:T(8,128)(2,1)S(1)}, bf16[512,512]{1,0:T(8,128)(2,1)S(1)}, u32[]{:S(2)}, u32[]{:S(2)}) collective-permute-start(bf16[512,512]{1,0:T(8,128)(2,1)S(1)} %add_convert_fusion.2), channel_id=1, source_target_pairs={{0,1},{1,2},{2,3},{3,0},{4,5},{5,6},{6,7},{7,4},{8,9},{9,10},{10,1... | collective-permute-start | bytes 1572872 | tf_op jit(solution)/shard_map/ppermute | solution.py:27
  239.4 8.6 %collective-permute-start.5 = (bf16[512,512]{1,0:T(8,128)(2,1)S(1)}, bf16[512,512]{1,0:T(8,128)(2,1)S(1)}, u32[]{:S(2)}, u32[]{:S(2)}) collective-permute-start(bf16[512,512]{1,0:T(8,128)(2,1)S(1)} %collective-permute-done.4), channel_id=1, source_target_pairs={{0,1},{1,2},{2,3},{3,0},{4,5},{5,6},{6,7},{7,4},{8,9},{9,10},{10,1... | collective-permute-start | bytes 1572872 | tf_op jit(solution)/shard_map/ppermute | solution.py:27
  248.0 8.6 %collective-permute-start.6 = (bf16[512,512]{1,0:T(8,128)(2,1)S(1)}, bf16[512,512]{1,0:T(8,128)(2,1)S(1)}, u32[]{:S(2)}, u32[]{:S(2)}) collective-permute-start(bf16[512,512]{1,0:T(8,128)(2,1)S(1)} %collective-permute-done.5), channel_id=1, source_target_pairs={{0,1},{1,2},{2,3},{3,0},{4,5},{5,6},{6,7},{7,4},{8,9},{9,10},{10,1... | collective-permute-start | bytes 1572872 | tf_op jit(solution)/shard_map/ppermute | solution.py:27
  266.4 4.8 %collective-permute-start.7 = (bf16[30,256]{1,0:T(8,128)(2,1)S(1)}, bf16[30,256]{1,0:T(8,128)(2,1)S(1)}, u32[]{:S(2)}, u32[]{:S(2)}) collective-permute-start(bf16[30,256]{1,0:T(8,128)(2,1)S(1)} %slice.880), channel_id=1, source_target_pairs={{0,4},{4,8},{8,12},{12,16},{16,20},{20,24},{24,28},{1,5},{5,9},{9,... | collective-permute-start | bytes 46088 | tf_op jit(solution)/shard_map/ppermute | solution.py:10
  282.9 117.7 %reduce-scatter.8.cloned.1.call-start = ((), (), s32[]{:S(2)}) async-start(), calls=%async_computation.8 | async-start | bytes 2621440 | tf_op jit(solution)/shard_map/reduce_scatter | solution.py:57
  316.3 8.7 %collective-permute-start.8 = (bf16[512,512]{1,0:T(8,128)(2,1)S(1)}, bf16[512,512]{1,0:T(8,128)(2,1)S(1)}, u32[]{:S(2)}, u32[]{:S(2)}) collective-permute-start(bf16[512,512]{1,0:T(8,128)(2,1)S(1)} %add_convert_fusion.1), channel_id=1, source_target_pairs={{0,1},{1,2},{2,3},{3,0},{4,5},{5,6},{6,7},{7,4},{8,9},{9,10},{10,1... | collective-permute-start | bytes 1572872 | tf_op jit(solution)/shard_map/ppermute | solution.py:27
  324.9 8.6 %collective-permute-start.9 = (bf16[512,512]{1,0:T(8,128)(2,1)S(1)}, bf16[512,512]{1,0:T(8,128)(2,1)S(1)}, u32[]{:S(2)}, u32[]{:S(2)}) collective-permute-start(bf16[512,512]{1,0:T(8,128)(2,1)S(1)} %collective-permute-done.8), channel_id=1, source_target_pairs={{0,1},{1,2},{2,3},{3,0},{4,5},{5,6},{6,7},{7,4},{8,9},{9,10},{10,1... | collective-permute-start | bytes 1572872 | tf_op jit(solution)/shard_map/ppermute | solution.py:27
  333.5 8.6 %collective-permute-start.10 = (bf16[512,512]{1,0:T(8,128)(2,1)S(1)}, bf16[512,512]{1,0:T(8,128)(2,1)S(1)}, u32[]{:S(2)}, u32[]{:S(2)}) collective-permute-start(bf16[512,512]{1,0:T(8,128)(2,1)S(1)} %collective-permute-done.9), channel_id=1, source_target_pairs={{0,1},{1,2},{2,3},{3,0},{4,5},{5,6},{6,7},{7,4},{8,9},{9,10},{10,1... | collective-permute-start | bytes 1572872 | tf_op jit(solution)/shard_map/ppermute | solution.py:27
  351.9 4.8 %collective-permute-start.11 = (bf16[30,256]{1,0:T(8,128)(2,1)S(1)}, bf16[30,256]{1,0:T(8,128)(2,1)S(1)}, u32[]{:S(2)}, u32[]{:S(2)}) collective-permute-start(bf16[30,256]{1,0:T(8,128)(2,1)S(1)} %slice.942), channel_id=1, source_target_pairs={{0,4},{4,8},{8,12},{12,16},{16,20},{20,24},{24,28},{1,5},{5,9},{9,... | collective-permute-start | bytes 46088 | tf_op jit(solution)/shard_map/ppermute | solution.py:10
Sparse Core Ops, SparseCore 0:
  9.5 62.7 all-gather.5
  74.5 58.6 all-gather.3
  135.2 61.3 all-gather.7
  200.1 29.3 reduce-scatter.3
  283.0 31.9 reduce-scatter.5
  368.6 31.9 reduce-scatter.7
